TPU v7x, 32 devices: a whole 2x2x4 slice. The times are simulated.
32 devices in a mesh: sp: 4 (over z), dp: 8 (over y, x, core).
Axes of the slice: x: 2, y: 2, z: 4, core: 2. Of those that a mesh axis runs over, the one named last changes fastest.
Arguments:
- probe_vectors: bfloat16 [4096, 1024], P(('dp', 'sp')), may hold values from -6 to 6
- address_vectors: bfloat16 [4096, 1024], P(('dp', 'sp')), may hold values from -6 to 6
- content_vectors: bfloat16 [4096, 2048], P(('dp', 'sp')), may hold values from -6 to 6
- adjoint_of_result: bfloat16 [4096, 2048], P(('dp', 'sp')), may hold values from -0.5 to 0.5
- compact_factor: bfloat16 [4096, 64], P(('dp', 'sp')), may hold values from -7.5 to 7.5
- latent_to_damping_map: bfloat16 [64, 1024], replicated, may hold values from -0.75 to 0.75
- damping_shift_term: float32 [1024], replicated
- surplus_damping: bfloat16 [4096, 16], P(('dp', 'sp')), may hold values from -0.7 to 0
Outputs:
- query_grad: bfloat16 [4096, 1024], P(('dp', 'sp'))
- key_grad: bfloat16 [4096, 1024], P(('dp', 'sp'))
- value_grad: bfloat16 [4096, 2048], P(('dp', 'sp'))
- latent_grad: bfloat16 [4096, 64], P(('dp', 'sp'))
- weight_grad: float32 [64, 1024], replicated
All inputs are finite; a program needn't handle non-finite values.
Results may differ from a plain program's by a relative error of at most 0.005.
Values may be sent and summed in bfloat16 or wider, within the bound.
No kernel may reach another device: no remote copies, remote signals or barrier semaphores. Data moves between devices by JAX's collectives and lax.ppermute only.
A program may use at most 64 MiB of HBM per device.

v0:
```python
import jax
import jax.numpy as jnp
from jax import lax
from jax.sharding import PartitionSpec as P

KEY_CHANNELS = 64
VALUE_DIM = 128
BLOCK = 64
gate_norm = 16.0
highest = lax.Precision.HIGHEST


def carry_states(block_total, increments):
    log_totals = block_total[:, :, 0, :]
    running = jnp.cumsum(log_totals, axis=1)
    before = running - log_totals
    blocks = log_totals.shape[1]
    order = jnp.arange(blocks, dtype=jnp.int32)
    earlier_mask = (order[None, :] < order[:, None])[None, :, :, None]
    exponent = before[:, :, None, :] - running[:, None, :, :]
    exponent = jnp.where(earlier_mask, exponent, jnp.zeros_like(exponent))
    weights = jnp.where(earlier_mask, jnp.exp(exponent), jnp.zeros_like(exponent))
    return jnp.einsum("hnmk,mhkv->nhkv", weights, increments, precision=highest)


def gla_forward(probe_vectors, address_vectors, content_vectors, logarithm_decay):
    head_count, seq_len, key_width = probe_vectors.shape
    value_width = content_vectors.shape[2]
    blocks = seq_len // BLOCK

    def blocked(tensor):
        return tensor.reshape(head_count, blocks, BLOCK, tensor.shape[2])

    cumulative = jnp.cumsum(blocked(logarithm_decay), axis=2)
    block_total = cumulative[:, :, BLOCK - 1 :, :]
    keys_block = blocked(address_vectors)
    query_decayed = blocked(probe_vectors) * key_width ** (-0.5) * jnp.exp(cumulative)
    key_inverse = keys_block * jnp.exp(-cumulative)
    key_to_end = keys_block * jnp.exp(block_total - cumulative)
    value_block = blocked(content_vectors)
    scores = jnp.einsum("hnik,hnjk->hnij", query_decayed, key_inverse, precision=highest)
    positions = jnp.arange(BLOCK, dtype=jnp.int32)
    causal = positions[:, None] >= positions[None, :]
    scores = jnp.where(causal, scores, jnp.zeros_like(scores))
    within_block = jnp.einsum("hnij,hnjv->hniv", scores, value_block, precision=highest)
    increments = jnp.einsum("hnjk,hnjv->nhkv", key_to_end, value_block, precision=highest)
    earlier = carry_states(block_total, increments)
    carried = jnp.einsum("hnik,nhkv->hniv", query_decayed, earlier, precision=highest)
    return (within_block + carried).reshape(head_count, seq_len, value_width)


def split_into_heads(tensor, width):
    return tensor.astype(jnp.float32).reshape(tensor.shape[0], -1, width).transpose(1, 0, 2)


def to_rows(tensor):
    return tensor.transpose(1, 0, 2).reshape(tensor.shape[1], tensor.shape[0] * tensor.shape[2])


def on_device(
    probe_vectors,
    address_vectors,
    content_vectors,
    adjoint_of_result,
    compact_factor,
    latent_to_damping_map,
    damping_shift_term,
    surplus_damping,
):
    query_per_head, key_per_head, value_per_head, upstream_heads, spike_heads = (
        lax.all_to_all(probe_vectors, "sp", split_axis=1, concat_axis=0, tiled=True),
        lax.all_to_all(address_vectors, "sp", split_axis=1, concat_axis=0, tiled=True),
        lax.all_to_all(content_vectors, "sp", split_axis=1, concat_axis=0, tiled=True),
        lax.all_to_all(adjoint_of_result, "sp", split_axis=1, concat_axis=0, tiled=True),
        lax.all_to_all(surplus_damping, "sp", split_axis=1, concat_axis=0, tiled=True),
    )
    local_width = query_per_head.shape[1]
    hidden_code_rows = lax.all_gather(compact_factor, "sp", axis=0, tiled=True)
    column_start = lax.axis_index("sp") * local_width
    weight_local = lax.dynamic_slice_in_dim(latent_to_damping_map, column_start, local_width, 1)
    bias_local = lax.dynamic_slice_in_dim(damping_shift_term, column_start, local_width, 0)
    gate_logit = (
        jnp.dot(hidden_code_rows, weight_local, preferred_element_type=jnp.float32) + bias_local
    )
    forget_rate_rows = jax.nn.log_sigmoid(gate_logit) / gate_norm
    logarithm_decay = (
        split_into_heads(forget_rate_rows, KEY_CHANNELS)
        + spike_heads.astype(jnp.float32).T[:, :, None]
    )
    _, pullback = jax.vjp(
        gla_forward,
        split_into_heads(query_per_head, KEY_CHANNELS),
        split_into_heads(key_per_head, KEY_CHANNELS),
        split_into_heads(value_per_head, VALUE_DIM),
        logarithm_decay,
    )
    grad_query, grad_key, grad_value, grad_decay = pullback(
        split_into_heads(upstream_heads, VALUE_DIM)
    )
    query_grad, key_grad, value_grad = (
        lax.all_to_all(
            to_rows(grad_query).astype(jnp.bfloat16), "sp", split_axis=0, concat_axis=1, tiled=True
        ),
        lax.all_to_all(
            to_rows(grad_key).astype(jnp.bfloat16), "sp", split_axis=0, concat_axis=1, tiled=True
        ),
        lax.all_to_all(
            to_rows(grad_value).astype(jnp.bfloat16), "sp", split_axis=0, concat_axis=1, tiled=True
        ),
    )
    decay_rows = to_rows(grad_decay)
    gate_grad = (decay_rows * jax.nn.sigmoid(-gate_logit) / gate_norm).astype(jnp.bfloat16)
    partial_latent = jnp.einsum(
        "sc,rc->sr", gate_grad, weight_local, preferred_element_type=jnp.float32
    )
    latent_grad = lax.psum_scatter(partial_latent, "sp", scatter_dimension=0, tiled=True).astype(
        jnp.bfloat16
    )
    local_weight = jnp.einsum(
        "sr,sc->rc", hidden_code_rows, gate_grad, preferred_element_type=jnp.float32
    )
    summed = lax.psum(local_weight, "dp")
    weight_grad = lax.all_gather(summed, "sp", axis=1, tiled=True)
    return (query_grad, key_grad, value_grad, latent_grad, weight_grad)


def solution(mesh):
    return jax.shard_map(
        on_device,
        mesh=mesh,
        in_specs=(
            P(("dp", "sp"), None),
            P(("dp", "sp"), None),
            P(("dp", "sp"), None),
            P(("dp", "sp"), None),
            P(("dp", "sp"), None),
            P(),
            P(),
            P(("dp", "sp"), None),
        ),
        out_specs=(
            P(("dp", "sp"), None),
            P(("dp", "sp"), None),
            P(("dp", "sp"), None),
            P(("dp", "sp"), None),
            P(),
        ),
        check_vma=False,
    )
```

profile of v0, /device:TPU:0, one launch (start us, length us, event | category | flops | bytes accessed | tf_op | source)
XLA Modules:
  0.0 277.0 jit_solution(3052615414394250195)
XLA Ops:
  8.0 6.5 %all-to-all-start.1 = ((bf16[128,4,4]{0,2,1:T(4,128)(2,1)}), bf16[128,4,4]{0,2,1:T(4,128)(2,1)S(1)}, u32[]{:S(2)}, u32[]{:S(2)}) async-start(bf16[128,4,4]{0,2,1:T(4,128)(2,1)} %bitcast.169), calls=%async_computation.1 | async-start | bytes 8192 | tf_op jit(solution)/shard_map/all_to_all | solution.py:75
  14.5 1.8 copy.214
  16.3 3.8 %all-to-all-done.1 = bf16[128,4,4]{0,2,1:T(4,128)(2,1)S(1)} async-done(((bf16[128,4,4]{0,2,1:T(4,128)(2,1)}), bf16[128,4,4]{0,2,1:T(4,128)(2,1)S(1)}, u32[]{:S(2)}, u32[]{:S(2)}) %all-to-all-start.1) | async-done | bytes 4128 | tf_op jit(solution)/shard_map/all_to_all | solution.py:75
  20.1 3.5 %all-to-all-start.5 = ((bf16[128,4,256]{0,2,1:T(8,128)(2,1)}), bf16[128,4,256]{0,2,1:T(8,128)(2,1)S(1)}, u32[]{:S(2)}, u32[]{:S(2)}) async-start(bf16[128,4,256]{0,2,1:T(8,128)(2,1)} %bitcast.24), calls=%async_computation.5 | async-start | bytes 524288 | tf_op jit(solution)/shard_map/all_to_all | solution.py:71
  24.5 7.0 %all-to-all-done.5 = bf16[128,4,256]{0,2,1:T(8,128)(2,1)S(1)} async-done(((bf16[128,4,256]{0,2,1:T(8,128)(2,1)}), bf16[128,4,256]{0,2,1:T(8,128)(2,1)S(1)}, u32[]{:S(2)}, u32[]{:S(2)}) %all-to-all-start.5) | async-done | bytes 262176 | tf_op jit(solution)/shard_map/all_to_all | solution.py:71
  31.5 3.4 %all-to-all-start = ((bf16[128,4,256]{0,2,1:T(8,128)(2,1)}), bf16[128,4,256]{0,2,1:T(8,128)(2,1)S(1)}, u32[]{:S(2)}, u32[]{:S(2)}) async-start(bf16[128,4,256]{0,2,1:T(8,128)(2,1)} %bitcast), calls=%async_computation | async-start | bytes 524288 | tf_op jit(solution)/shard_map/all_to_all | solution.py:72
  36.6 12.5 %all_gather.6 = bf16[512,64]{0,1:T(8,128)(2,1)S(1)} all-gather(bf16[128,64]{0,1:T(8,128)(2,1)S(1)} %copy-done.31), channel_id=1, replica_groups=mesh['sp'=4,'dp'=8] {'sp'}, dimensions={0}, use_global_device_ids=true | all-gather | bytes 81920 | tf_op jit(solution)/shard_map/all_gather | solution.py:78
  49.7 1.3 fusion.20
  51.7 4.1 %all-to-all-start.3 = ((bf16[128,4,512]{2,0,1:T(8,128)(2,1)}), bf16[128,4,512]{2,0,1:T(8,128)(2,1)}, u32[]{:S(2)}, u32[]{:S(2)}) async-start(bf16[128,4,512]{2,0,1:T(8,128)(2,1)} %bitcast.143), calls=%async_computation.3 | async-start | bytes 1048576 | tf_op jit(solution)/shard_map/all_to_all | solution.py:74
  56.4 0.9 copy.312
  58.0 25.9 %fusion.46 = f32[4,8,64,64]{3,1,2,0:T(8,128)S(1)} fusion(f32[4,8,64,64]{3,1,2,0:T(8,128)S(1)} %copy.194), kind=kOutput, calls=%fused_computation.84 | output fusion | flops 8257536 | bytes 1048576 | tf_op jit(solution)/shard_map/jvp(jit(cumsum))/reduce_window_sum | solution.py:34
  83.9 5.1 %all-to-all-start.2 = ((bf16[128,4,512]{2,0,1:T(8,128)(2,1)}), bf16[128,4,512]{2,0,1:T(8,128)(2,1)}, u32[]{:S(2)}, u32[]{:S(2)}) async-start(bf16[128,4,512]{2,0,1:T(8,128)(2,1)} %bitcast.144), calls=%async_computation.2 | async-start | bytes 1048576 | tf_op jit(solution)/shard_map/all_to_all | solution.py:73
  92.8 1.0 reshape.170
  93.8 1.2 reshape.166
  95.1 2.0 reshape.161
  97.0 1.9 copy.205
  99.4 2.0 reshape.159
  101.3 1.2 copy.198
  102.6 0.9 convolution_bitcast_fusion.3
  103.7 2.9 %convolution_bitcast_fusion = f32[8,4,64,128]{3,0,2,1:T(8,128)S(1)} fusion(f32[4,64,128,8]{2,1,3,0:T(8,128)S(1)} %convolution_bitcast_fusion.3, f32[4,8,64]{1,2,0:T(8,128)S(1)} %copy-done.23, f32[4,8,64]{1,2,0:T(8,128)S(1)} %copy-done.24, pred[8,8]{1,0:T(8,128)(4,1)S(1)} %copy-done.32), kind=kOutput, calls=%fused_computation.4 | convolution fusion | flops 25214976 | bytes 2113600 | tf_op jit(solution)/shard_map/transpose(jvp(hnmk,mhkv->nhkv))/dot_general | solution.py:23
  106.6 2.8 %fusion.18 = (f32[4,8,64]{2,1,0:T(8,128)}, f32[4,8,64,64]{2,3,1,0:T(8,128)S(1)}, f32[4,8,64,64]{2,3,1,0:T(8,128)}) fusion(f32[4,8,64,64]{2,3,1,0:T(8,128)S(1)} %copy.195, f32[4,8,64,64]{2,1,3,0:T(8,128)S(1)} %reshape.166, f32[4,8,64]{2,1,0:T(8,128)S(1)} %slice_bitcast_fusion, bf16[4,8,64,128]{3,2,1,0:T(8,128)(2,1)S(1)} %bitcast.150, ...), kind=kOutput, calls=%fused_computation.40 | convolution fusion | flops 201979904 | bytes 3686400 | tf_op jit(solution)/shard_map/transpose(jvp(hnjk,hnjv->nhkv))/dot_general | solution.py:46
  110.4 2.5 convolution_bitcast_fusion.1
  112.9 4.3 %fusion.45 = (f32[4,8,64]{1,2,0:T(8,128)}, f32[4,8,64]{1,2,0:T(8,128)}) fusion(f32[4,8,64]{1,2,0:T(8,128)S(1)} %copy-done.23, f32[4,8,64]{1,2,0:T(8,128)S(1)} %copy-done.24, f32[8,4,64,128]{3,2,1,0:T(8,128)S(1)} %fusion.6, f32[4,64,128,8]{2,1,3,0:T(8,128)S(1)} %convolution_bitcast_fusion.3, pred[8,8]{1,0:T(8,128)(4,1)S(1)} %copy-done.32), kind=kOutput, calls=%fused_computation.83 | convolution fusion | flops 25276416 | bytes 2129984 | tf_op jit(solution)/shard_map/transpose(jvp(hnmk,mhkv->nhkv))/dot_general | solution.py:23
  117.3 2.0 convolution_bitcast_fusion.4
  120.9 1.4 copy.243
  122.2 1.4 copy.244
  123.6 1.4 copy.245
  125.1 1.6 convolution_select_fusion
  126.7 1.3 fusion.44
  128.6 1.5 fusion.3
  130.1 3.7 %pad_add_fusion = (f32[4,8,64,64]{2,3,1,0:T(8,128)}, bf16[4,8,64,64]{2,3,1,0:T(8,128)(2,1)}, bf16[4,8,64,64]{2,3,1,0:T(8,128)(2,1)S(1)}) fusion(f32[4,8,1,64]{2,3,1,0:T(8,128)S(1)} %fusion.3, f32[4,8,64,64]{2,3,1,0:T(8,128)S(1)} %fusion.44, f32[4,8,64,64]{2,1,3,0:T(8,128)S(1)} %mul.72, f32[4,8,64,64]{2,3,1,0:T(8,128)S(1)} %copy.195, ...), kind=kOutput, calls=%fused_computation.22 | convolution fusion | flops 103677952 | bytes 4734976 | tf_op jit(solution)/shard_map/transpose(jvp(hnik,hnjk->hnij))/dot_general | solution.py:41
  133.8 1.1 copy.212
  134.9 1.4 convert_element_type.73
  137.1 1.7 copy.213
  138.8 4.8 %all-to-all-start.4 = ((bf16[4,128,256]{1,2,0:T(8,128)(2,1)}), bf16[4,128,256]{1,2,0:T(8,128)(2,1)S(1)}, u32[]{:S(2)}, u32[]{:S(2)}) async-start(bf16[4,128,256]{1,2,0:T(8,128)(2,1)} %copy.213), calls=%async_computation.4 | async-start | bytes 524288 | tf_op jit(solution)/shard_map/all_to_all | solution.py:101
  143.6 3.1 %convolution_select_fusion.2 = f32[4,8,64,64]{3,2,1,0:T(8,128)} fusion(pred[64,64]{1,0:T(8,128)(4,1)S(1)} %copy-done.28, f32[4,8,64,64]{2,1,3,0:T(8,128)S(1)} %reshape.166, f32[4,8,64,64]{2,3,1,0:T(8,128)S(1)} %copy.195, f32[4,8,64,64]{2,1,3,0:T(8,128)S(1)} %mul.72), kind=kOutput, calls=%fused_computation.11 | convolution fusion | flops 101187584 | bytes 2101248 | tf_op jit(solution)/shard_map/jvp(hnik,hnjk->hnij)/dot_general | solution.py:41
  148.3 3.2 %fusion.11 = f32[4,8,64,128]{3,2,1,0:T(8,128)S(1)} fusion(f32[4,8,64,64]{2,3,1,0:T(8,128)S(1)} %copy-done.4, f32[8,4,64,128]{3,0,2,1:T(8,128)} %copy-done.9), kind=kOutput, calls=%fused_computation.30 | convolution fusion | flops 201326592 | bytes 2621440 | tf_op jit(solution)/shard_map/transpose(jvp(hnjk,hnjv->nhkv))/dot_general | solution.py:46
  151.5 5.2 %all-to-all-start.6 = ((bf16[4,128,256]{1,2,0:T(8,128)(2,1)}), bf16[4,128,256]{1,2,0:T(8,128)(2,1)S(1)}, u32[]{:S(2)}, u32[]{:S(2)}) async-start(bf16[4,128,256]{1,2,0:T(8,128)(2,1)} %copy.226), calls=%async_computation.6 | async-start | bytes 524288 | tf_op jit(solution)/shard_map/all_to_all | solution.py:104
  156.7 1.0 fusion.4
  158.2 1.0 convert_element_type.84
  159.6 25.8 %fusion.47 = f32[4,8,64,64]{3,1,2,0:T(8,128)S(1)} fusion(f32[4,8,64,64]{3,1,2,0:T(8,128)S(1)} %copy.246), kind=kOutput, calls=%fused_computation.85 | output fusion | flops 8257536 | bytes 1048576 | tf_op jit(solution)/shard_map/transpose(jvp(jit(cumsum)))/reduce_window_sum | solution.py:34
  186.1 5.2 %all-to-all-start.7 = ((bf16[4,128,512]{2,1,0:T(8,128)(2,1)}), bf16[4,128,512]{2,1,0:T(8,128)(2,1)S(1)}, u32[]{:S(2)}, u32[]{:S(2)}) async-start(bf16[4,128,512]{2,1,0:T(8,128)(2,1)} %convert_element_type.84), calls=%async_computation.7 | async-start | bytes 1048576 | tf_op jit(solution)/shard_map/all_to_all | solution.py:107
  193.9 56.5 %all-reduce.3.cloned.1.call-done = f32[64,256]{1,0:T(8,128)} async-done(((f32[64,256]{1,0:T(8,128)}), f32[64,256]{1,0:T(8,128)}) %all-reduce.3.cloned.1.call-update) | async-done | bytes 65552 | tf_op jit(solution)/shard_map/psum | solution.py:122
  250.4 14.1 %all_gather.7 = f32[64,1024]{1,0:T(8,128)S(1)} all-gather(f32[64,256]{1,0:T(8,128)} %all-reduce.3.cloned.1.call-done), channel_id=1, replica_groups=mesh['sp'=4,'dp'=8] {'sp'}, dimensions={1}, use_global_device_ids=true | all-gather | bytes 327680 | tf_op jit(solution)/shard_map/all_gather | solution.py:123
  264.5 1.4 convert_element_type.86
  265.9 0.8 copy.248
  266.7 0.8 copy.249
  267.9 1.0 copy.250
  (116 shorter events, 20.1 us)
Async XLA Ops:
  8.0 41.7 %copy-start = (bf16[64,1024]{1,0:T(8,128)(2,1)S(1)}, bf16[64,1024]{1,0:T(8,128)(2,1)}, u32[]{:S(2)}) copy-start(bf16[64,1024]{1,0:T(8,128)(2,1)} %param.13) | copy-start | bytes 393220
  8.0 12.1 %all-to-all-start.1 = ((bf16[128,4,4]{0,2,1:T(4,128)(2,1)}), bf16[128,4,4]{0,2,1:T(4,128)(2,1)S(1)}, u32[]{:S(2)}, u32[]{:S(2)}) async-start(bf16[128,4,4]{0,2,1:T(4,128)(2,1)} %bitcast.169), calls=%async_computation.1 | async-start | bytes 8192 | tf_op jit(solution)/shard_map/all_to_all | solution.py:75
  20.1 3.6 %copy-start.20 = (bf16[128,1024]{1,0:T(8,128)(2,1)S(1)}, bf16[128,1024]{1,0:T(8,128)(2,1)}, u32[]{:S(2)}) copy-start(bf16[128,1024]{1,0:T(8,128)(2,1)} %param.9) | copy-start | bytes 786436
  20.1 11.4 %all-to-all-start.5 = ((bf16[128,4,256]{0,2,1:T(8,128)(2,1)}), bf16[128,4,256]{0,2,1:T(8,128)(2,1)S(1)}, u32[]{:S(2)}, u32[]{:S(2)}) async-start(bf16[128,4,256]{0,2,1:T(8,128)(2,1)} %bitcast.24), calls=%async_computation.5 | async-start | bytes 524288 | tf_op jit(solution)/shard_map/all_to_all | solution.py:71
  23.6 11.3 %copy-start.17 = (bf16[128,2048]{1,0:T(8,128)(2,1)S(1)}, bf16[128,2048]{1,0:T(8,128)(2,1)}, u32[]{:S(2)}) copy-start(bf16[128,2048]{1,0:T(8,128)(2,1)} %param.11) | copy-start | bytes 1572868
  31.5 19.5 %all-to-all-start = ((bf16[128,4,256]{0,2,1:T(8,128)(2,1)}), bf16[128,4,256]{0,2,1:T(8,128)(2,1)S(1)}, u32[]{:S(2)}, u32[]{:S(2)}) async-start(bf16[128,4,256]{0,2,1:T(8,128)(2,1)} %bitcast), calls=%async_computation | async-start | bytes 524288 | tf_op jit(solution)/shard_map/all_to_all | solution.py:72
  35.0 1.6 copy-start.31
  49.0 1.9 copy-start.21
  51.0 0.7 copy-start.15
  51.0 5.4 %copy-start.18 = (bf16[128,2048]{1,0:T(8,128)(2,1)S(1)}, bf16[128,2048]{1,0:T(8,128)(2,1)}, u32[]{:S(2)}) copy-start(bf16[128,2048]{1,0:T(8,128)(2,1)} %param.10) | copy-start | bytes 1572868
  51.7 32.2 %all-to-all-start.3 = ((bf16[128,4,512]{2,0,1:T(8,128)(2,1)}), bf16[128,4,512]{2,0,1:T(8,128)(2,1)}, u32[]{:S(2)}, u32[]{:S(2)}) async-start(bf16[128,4,512]{2,0,1:T(8,128)(2,1)} %bitcast.143), calls=%async_computation.3 | async-start | bytes 1048576 | tf_op jit(solution)/shard_map/all_to_all | solution.py:74
  83.9 15.5 %all-to-all-start.2 = ((bf16[128,4,512]{2,0,1:T(8,128)(2,1)}), bf16[128,4,512]{2,0,1:T(8,128)(2,1)}, u32[]{:S(2)}, u32[]{:S(2)}) async-start(bf16[128,4,512]{2,0,1:T(8,128)(2,1)} %bitcast.144), calls=%async_computation.2 | async-start | bytes 1048576 | tf_op jit(solution)/shard_map/all_to_all | solution.py:73
  91.5 1.0 copy-start.16
  101.3 1.2 copy-start.1
  102.5 7.0 %copy-start.5 = (bf16[4,512,128]{2,1,0:T(8,128)(2,1)}, bf16[4,512,128]{2,1,0:T(8,128)(2,1)S(1)}, u32[]{:S(2)}) copy-start(bf16[4,512,128]{2,1,0:T(8,128)(2,1)S(1)} %copy.198) | copy-start | bytes 1572868
  102.5 1.1 copy-start.23
  102.5 1.1 copy-start.24
  102.5 1.1 copy-start.32
  106.6 2.9 %copy-start.9 = (f32[8,4,64,128]{3,0,2,1:T(8,128)}, f32[8,4,64,128]{3,0,2,1:T(8,128)S(1)}, u32[]{:S(2)}) copy-start(f32[8,4,64,128]{3,0,2,1:T(8,128)S(1)} %convolution_bitcast_fusion) | copy-start | bytes 3145732
  109.5 1.0 copy-start.3
  117.3 2.0 copy-start.26
  119.2 0.9 copy-start.25
  120.1 0.7 copy-start.30
  122.2 1.4 copy-start.29
  123.6 1.4 copy-start.27
  126.7 1.3 copy-start.11
  126.7 1.5 copy-start.12
  126.7 1.8 copy-start.13
  128.5 1.5 copy-start.8
  128.5 1.5 copy-start.10
  138.8 4.8 %copy-start.28 = (pred[64,64]{1,0:T(8,128)(4,1)S(1)}, pred[64,64]{1,0:T(8,128)(4,1)}, u32[]{:S(2)}) copy-start(pred[64,64]{1,0:T(8,128)(4,1)} %iota_compare_fusion) | copy-start | bytes 12292
  138.8 12.7 %all-to-all-start.4 = ((bf16[4,128,256]{1,2,0:T(8,128)(2,1)}), bf16[4,128,256]{1,2,0:T(8,128)(2,1)S(1)}, u32[]{:S(2)}, u32[]{:S(2)}) async-start(bf16[4,128,256]{1,2,0:T(8,128)(2,1)} %copy.213), calls=%async_computation.4 | async-start | bytes 524288 | tf_op jit(solution)/shard_map/all_to_all | solution.py:101
  143.6 3.1 %copy-start.14 = (bf16[4,8,64,64]{2,3,1,0:T(8,128)(2,1)S(1)}, bf16[4,8,64,64]{2,3,1,0:T(8,128)(2,1)}, u32[]{:S(2)}) copy-start(bf16[4,8,64,64]{2,3,1,0:T(8,128)(2,1)} %get-tuple-element.23) | copy-start | bytes 786436
  147.1 1.2 copy-start.4
  148.3 8.4 %copy-start.6 = (f32[4,8,64,64]{3,2,1,0:T(8,128)S(1)}, f32[4,8,64,64]{3,2,1,0:T(8,128)}, u32[]{:S(2)}) copy-start(f32[4,8,64,64]{3,2,1,0:T(8,128)} %convolution_select_fusion.2) | copy-start | bytes 1572868
  151.5 5.3 %copy-start.2 = (bf16[4,512,128]{2,1,0:T(8,128)(2,1)S(1)}, bf16[4,512,128]{2,1,0:T(8,128)(2,1)}, u32[]{:S(2)}) copy-start(bf16[4,512,128]{2,1,0:T(8,128)(2,1)} %copy.205) | copy-start | bytes 1572868
  151.5 34.6 %all-to-all-start.6 = ((bf16[4,128,256]{1,2,0:T(8,128)(2,1)}), bf16[4,128,256]{1,2,0:T(8,128)(2,1)S(1)}, u32[]{:S(2)}, u32[]{:S(2)}) async-start(bf16[4,128,256]{1,2,0:T(8,128)(2,1)} %copy.226), calls=%async_computation.6 | async-start | bytes 524288 | tf_op jit(solution)/shard_map/all_to_all | solution.py:104
  157.7 1.4 copy-start.7
  186.1 5.3 %copy-start.19 = (f32[256,512]{1,0:T(8,128)S(1)}, f32[256,512]{1,0:T(8,128)}, u32[]{:S(2)}) copy-start(f32[256,512]{1,0:T(8,128)} %get-tuple-element.30) | copy-start | bytes 1572868
  186.1 81.5 %all-to-all-start.7 = ((bf16[4,128,512]{2,1,0:T(8,128)(2,1)}), bf16[4,128,512]{2,1,0:T(8,128)(2,1)S(1)}, u32[]{:S(2)}, u32[]{:S(2)}) async-start(bf16[4,128,512]{2,1,0:T(8,128)(2,1)} %convert_element_type.84), calls=%async_computation.7 | async-start | bytes 1048576 | tf_op jit(solution)/shard_map/all_to_all | solution.py:107
  191.3 59.1 %all-reduce.3.cloned.1.call-start = ((), (), s32[]{:S(2)}) async-start(), calls=%async_computation.10 | async-start | bytes 131072 | tf_op jit(solution)/shard_map/psum | solution.py:122
  191.3 0.8 copy-start.22
  193.0 71.5 %reduce-scatter.2.cloned.1.call-start = ((), (), s32[]{:S(2)}) async-start(), calls=%async_computation.9 | async-start | bytes 163840 | tf_op jit(solution)/shard_map/reduce_scatter | solution.py:116
Sparse Core Ops, SparseCore 0:
  195.7 54.6 all-reduce.2
Sparse Core Ops, SparseCore 1:
  196.3 20.9 reduce-scatter.1
where the time goes:
time: 279 us; the launch traced here: 277 us
  waiting for transfers between devices  67.7 us (24%)
  other arithmetic  56 us (20%)
  local copies, waits for them, and re-layouts  39.8 us (14%)
  starting transfers between devices  38 us (14%)
  matrix products  32.9 us (12%)
  blocking collectives  26.6 us (10%)
  between operations  15.9 us (6%)
    psum x1, waiting for transfers between devices, on_device(): summed = lax.psum(local_weight, 'dp')  56.5 us
    another operation x2, other arithmetic, gla_forward(): cumulative = jnp.cumsum(blocked(logarithm_decay), axis=2)  51.6 us
    all_gather x1, blocking collectives, on_device(): weight_grad = lax.all_gather(summed, 'sp', axis=1, tiled=True)  14.1 us
    all_gather x1, blocking collectives, on_device(): hidden_code_rows = lax.all_gather(compact_factor, 'sp', axis=0, tiled=True)  12.5 us
    unnamed x72, local copies, waits for them, and re-layouts  10.3 us
    dot_general x3, matrix products, carry_states(): return jnp.einsum('hnmk,mhkv->nhkv', weights, increments, precision=highest)  9.75 us
    dot_general x3, matrix products, gla_forward(): jnp.einsum('hnik,hnjk->hnij', query_decayed, key_inverse, precision=highest)  8.12 us
    all_to_all x1, waiting for transfers between devices, on_device(): lax.all_to_all(probe_vectors, 'sp', split_axis=1, concat_axis=0, tiled=True)  7.02 us
  transfers between devices with their start and end apart: 10, of which 4 were waited for; matrix products, arithmetic and copies ran while one was open for 31% of the time, Pallas kernels for 0%

commit v1 on v0

--- a/solution.py
+++ b/solution.py
@@ -119,7 +119,9 @@
     local_weight = jnp.einsum(
         "sr,sc->rc", hidden_code_rows, gate_grad, preferred_element_type=jnp.float32
     )
-    summed = lax.psum(local_weight, "dp")
+    summed = local_weight
+    for hop in (1, 2, 4):
+        summed = summed + lax.ppermute(summed, "dp", [(dev, dev ^ hop) for dev in range(8)])
     weight_grad = lax.all_gather(summed, "sp", axis=1, tiled=True)
     return (query_grad, key_grad, value_grad, latent_grad, weight_grad)
 

time: 279 us -> 211 us (0.76)
  waiting for transfers between devices: 67.7 us -> 17.1 us
  other arithmetic: 56 us -> 32.6 us
  local copies, waits for them, and re-layouts: 39.8 us -> 45.5 us
  starting transfers between devices: 38 us -> 41 us
    psum x1 -> x0, waiting for transfers between devices: 56.5 us -> none  [on_device(): summed = lax.psum(local_weight, 'dp')]
    another operation x2, other arithmetic: 51.6 us -> 28.2 us  [gla_forward(): cumulative = jnp.cumsum(blocked(logarithm_decay), axis=2)]
    ppermute x0 -> x3, waiting for transfers between devices: none -> 5.9 us  [on_device(): lax.ppermute(summed, 'dp', [(dev, dev ^ hop) for dev in range(8)])]
    ppermute x0 -> x3, starting transfers between devices: none -> 3.22 us  [on_device(): lax.ppermute(summed, 'dp', [(dev, dev ^ hop) for dev in range(8)])]
  transfers between devices with their start and end apart: 10 -> 12, of which waited for: 4 -> 6; matrix products, arithmetic and copies ran while one was open for 31% -> 31% of each run, Pallas kernels for 0% -> 0%
where the time goes in v1:
time: 211 us; the launch traced here: 209 us
  local copies, waits for them, and re-layouts  45.5 us (22%)
  starting transfers between devices  41 us (19%)
  other arithmetic  32.6 us (15%)
  matrix products  31 us (15%)
  blocking collectives  27.8 us (13%)
  waiting for transfers between devices  17.1 us (8%)
  between operations  14.5 us (7%)
    another operation x2, other arithmetic, gla_forward(): cumulative = jnp.cumsum(blocked(logarithm_decay), axis=2)  28.2 us
    all_gather x1, blocking collectives, on_device(): weight_grad = lax.all_gather(summed, 'sp', axis=1, tiled=True)  15.3 us
    all_gather x1, blocking collectives, on_device(): hidden_code_rows = lax.all_gather(compact_factor, 'sp', axis=0, tiled=True)  12.5 us
    unnamed x72, local copies, waits for them, and re-layouts  11.4 us
    dot_general x3, matrix products, carry_states(): return jnp.einsum('hnmk,mhkv->nhkv', weights, increments, precision=highest)  9.75 us
    dot_general x3, matrix products, gla_forward(): jnp.einsum('hnik,hnjk->hnij', query_decayed, key_inverse, precision=highest)  8.16 us
    all_to_all x1, waiting for transfers between devices, on_device(): lax.all_to_all(probe_vectors, 'sp', split_axis=1, concat_axis=0, tiled=True)  7.02 us
    all_to_all x1, starting transfers between devices, on_device(): lax.all_to_all(surplus_damping, 'sp', split_axis=1, concat_axis=0, tiled=...  6.49 us
  transfers between devices with their start and end apart: 12, of which 6 were waited for; matrix products, arithmetic and copies ran while one was open for 31% of the time, Pallas kernels for 0%

profile of v1, /device:TPU:0, one launch (start us, length us, event | category | flops | bytes accessed | tf_op | source)
XLA Modules:
  0.0 209.5 jit_solution(167029506770008685)
XLA Ops:
  7.2 6.5 %all-to-all-start.1 = ((bf16[128,4,4]{0,2,1:T(4,128)(2,1)}), bf16[128,4,4]{0,2,1:T(4,128)(2,1)S(1)}, u32[]{:S(2)}, u32[]{:S(2)}) async-start(bf16[128,4,4]{0,2,1:T(4,128)(2,1)} %bitcast.168), calls=%async_computation.1 | async-start | bytes 8192 | tf_op jit(solution)/shard_map/all_to_all | solution.py:75
  13.7 1.8 copy.214
  15.5 3.8 %all-to-all-done.1 = bf16[128,4,4]{0,2,1:T(4,128)(2,1)S(1)} async-done(((bf16[128,4,4]{0,2,1:T(4,128)(2,1)}), bf16[128,4,4]{0,2,1:T(4,128)(2,1)S(1)}, u32[]{:S(2)}, u32[]{:S(2)}) %all-to-all-start.1) | async-done | bytes 4128 | tf_op jit(solution)/shard_map/all_to_all | solution.py:75
  19.3 3.5 %all-to-all-start.5 = ((bf16[128,4,256]{0,2,1:T(8,128)(2,1)}), bf16[128,4,256]{0,2,1:T(8,128)(2,1)S(1)}, u32[]{:S(2)}, u32[]{:S(2)}) async-start(bf16[128,4,256]{0,2,1:T(8,128)(2,1)} %bitcast.24), calls=%async_computation.5 | async-start | bytes 524288 | tf_op jit(solution)/shard_map/all_to_all | solution.py:71
  23.7 7.0 %all-to-all-done.5 = bf16[128,4,256]{0,2,1:T(8,128)(2,1)S(1)} async-done(((bf16[128,4,256]{0,2,1:T(8,128)(2,1)}), bf16[128,4,256]{0,2,1:T(8,128)(2,1)S(1)}, u32[]{:S(2)}, u32[]{:S(2)}) %all-to-all-start.5) | async-done | bytes 262176 | tf_op jit(solution)/shard_map/all_to_all | solution.py:71
  30.7 3.4 %all-to-all-start = ((bf16[128,4,256]{0,2,1:T(8,128)(2,1)}), bf16[128,4,256]{0,2,1:T(8,128)(2,1)S(1)}, u32[]{:S(2)}, u32[]{:S(2)}) async-start(bf16[128,4,256]{0,2,1:T(8,128)(2,1)} %bitcast), calls=%async_computation | async-start | bytes 524288 | tf_op jit(solution)/shard_map/all_to_all | solution.py:72
  35.7 12.5 %all_gather.6 = bf16[512,64]{0,1:T(8,128)(2,1)S(1)} all-gather(bf16[128,64]{0,1:T(8,128)(2,1)S(1)} %copy-done.31), channel_id=1, replica_groups=mesh['sp'=4,'dp'=8] {'sp'}, dimensions={0}, use_global_device_ids=true | all-gather | bytes 81920 | tf_op jit(solution)/shard_map/all_gather | solution.py:78
  48.8 1.3 fusion.20
  50.8 4.1 %all-to-all-start.3 = ((bf16[128,4,512]{2,0,1:T(8,128)(2,1)}), bf16[128,4,512]{2,0,1:T(8,128)(2,1)}, u32[]{:S(2)}, u32[]{:S(2)}) async-start(bf16[128,4,512]{2,0,1:T(8,128)(2,1)} %bitcast.143), calls=%async_computation.3 | async-start | bytes 1048576 | tf_op jit(solution)/shard_map/all_to_all | solution.py:74
  57.2 25.9 %fusion.46 = f32[4,8,64,64]{3,1,2,0:T(8,128)S(1)} fusion(f32[4,8,64,64]{3,1,2,0:T(8,128)S(1)} %copy.194), kind=kOutput, calls=%fused_computation.84 | output fusion | flops 8257536 | bytes 1048576 | tf_op jit(solution)/shard_map/jvp(jit(cumsum))/reduce_window_sum | solution.py:34
  83.1 5.1 %all-to-all-start.2 = ((bf16[128,4,512]{2,0,1:T(8,128)(2,1)}), bf16[128,4,512]{2,0,1:T(8,128)(2,1)}, u32[]{:S(2)}, u32[]{:S(2)}) async-start(bf16[128,4,512]{2,0,1:T(8,128)(2,1)} %bitcast.144), calls=%async_computation.2 | async-start | bytes 1048576 | tf_op jit(solution)/shard_map/all_to_all | solution.py:73
  93.0 1.2 reshape.166
  94.2 2.0 reshape.161
  96.2 1.9 copy.205
  98.5 2.0 reshape.159
  100.5 1.2 copy.198
  102.8 2.9 %convolution_bitcast_fusion = f32[8,4,64,128]{3,0,2,1:T(8,128)S(1)} fusion(f32[4,64,128,8]{2,1,3,0:T(8,128)S(1)} %convolution_bitcast_fusion.3, f32[4,8,64]{1,2,0:T(8,128)S(1)} %copy-done.23, f32[4,8,64]{1,2,0:T(8,128)S(1)} %copy-done.24, pred[8,8]{1,0:T(8,128)(4,1)S(1)} %copy-done.32), kind=kOutput, calls=%fused_computation.4 | convolution fusion | flops 25214976 | bytes 2113600 | tf_op jit(solution)/shard_map/transpose(jvp(hnmk,mhkv->nhkv))/dot_general | solution.py:23
  105.8 2.8 %fusion.18 = (f32[4,8,64]{2,1,0:T(8,128)}, f32[4,8,64,64]{2,3,1,0:T(8,128)S(1)}, f32[4,8,64,64]{2,3,1,0:T(8,128)}) fusion(f32[4,8,64,64]{2,3,1,0:T(8,128)S(1)} %copy.195, f32[4,8,64,64]{2,1,3,0:T(8,128)S(1)} %reshape.166, f32[4,8,64]{2,1,0:T(8,128)S(1)} %slice_bitcast_fusion, bf16[4,8,64,128]{3,2,1,0:T(8,128)(2,1)S(1)} %bitcast.150, ...), kind=kOutput, calls=%fused_computation.40 | convolution fusion | flops 201979904 | bytes 3686400 | tf_op jit(solution)/shard_map/transpose(jvp(hnjk,hnjv->nhkv))/dot_general | solution.py:46
  109.6 2.5 %convolution_bitcast_fusion.1 = f32[8,4,64,128]{3,0,2,1:T(8,128)S(1)} fusion(f32[8,4,64,128]{3,2,1,0:T(8,128)S(1)} %fusion.6, f32[4,8,64]{1,2,0:T(8,128)S(1)} %copy-done.23, f32[4,8,64]{1,2,0:T(8,128)S(1)} %copy-done.24, pred[8,8]{1,0:T(8,128)(4,1)S(1)} %copy-done.32), kind=kOutput, calls=%fused_computation.6 | convolution fusion | flops 25214976 | bytes 2113600 | tf_op jit(solution)/shard_map/jvp(hnmk,mhkv->nhkv)/dot_general | solution.py:23
  112.1 4.3 %fusion.45 = (f32[4,8,64]{1,2,0:T(8,128)}, f32[4,8,64]{1,2,0:T(8,128)}) fusion(f32[4,8,64]{1,2,0:T(8,128)S(1)} %copy-done.23, f32[4,8,64]{1,2,0:T(8,128)S(1)} %copy-done.24, f32[8,4,64,128]{3,2,1,0:T(8,128)S(1)} %fusion.6, f32[4,64,128,8]{2,1,3,0:T(8,128)S(1)} %convolution_bitcast_fusion.3, pred[8,8]{1,0:T(8,128)(4,1)S(1)} %copy-done.32), kind=kOutput, calls=%fused_computation.83 | convolution fusion | flops 25276416 | bytes 2129984 | tf_op jit(solution)/shard_map/transpose(jvp(hnmk,mhkv->nhkv))/dot_general | solution.py:23
  116.4 2.0 convolution_bitcast_fusion.4
  120.0 1.4 copy.243
  121.4 1.4 copy.244
  122.8 1.4 copy.245
  124.2 1.6 convolution_select_fusion
  125.9 1.3 fusion.44
  127.7 1.5 fusion.3
  129.2 3.7 %pad_add_fusion = (f32[4,8,64,64]{2,3,1,0:T(8,128)}, bf16[4,8,64,64]{2,3,1,0:T(8,128)(2,1)}, bf16[4,8,64,64]{2,3,1,0:T(8,128)(2,1)S(1)}) fusion(f32[4,8,1,64]{2,3,1,0:T(8,128)S(1)} %fusion.3, f32[4,8,64,64]{2,3,1,0:T(8,128)S(1)} %fusion.44, f32[4,8,64,64]{2,1,3,0:T(8,128)S(1)} %mul.72, f32[4,8,64,64]{2,3,1,0:T(8,128)S(1)} %copy.195, ...), kind=kOutput, calls=%fused_computation.22 | convolution fusion | flops 103677952 | bytes 4734976 | tf_op jit(solution)/shard_map/transpose(jvp(hnik,hnjk->hnij))/dot_general | solution.py:41
  133.0 1.1 copy.212
  134.1 1.4 convert_element_type.73
  136.3 1.7 copy.213
  138.0 4.9 %all-to-all-start.4 = ((bf16[4,128,256]{1,2,0:T(8,128)(2,1)}), bf16[4,128,256]{1,2,0:T(8,128)(2,1)S(1)}, u32[]{:S(2)}, u32[]{:S(2)}) async-start(bf16[4,128,256]{1,2,0:T(8,128)(2,1)} %copy.213), calls=%async_computation.4 | async-start | bytes 524288 | tf_op jit(solution)/shard_map/all_to_all | solution.py:101
  142.8 3.1 %convolution_select_fusion.2 = f32[4,8,64,64]{3,2,1,0:T(8,128)} fusion(pred[64,64]{1,0:T(8,128)(4,1)S(1)} %copy-done.28, f32[4,8,64,64]{2,1,3,0:T(8,128)S(1)} %reshape.166, f32[4,8,64,64]{2,3,1,0:T(8,128)S(1)} %copy.195, f32[4,8,64,64]{2,1,3,0:T(8,128)S(1)} %mul.72), kind=kOutput, calls=%fused_computation.11 | convolution fusion | flops 101187584 | bytes 2101248 | tf_op jit(solution)/shard_map/jvp(hnik,hnjk->hnij)/dot_general | solution.py:41
  146.0 2.6 %copy.246 = f32[4,8,64,64]{3,1,2,0:T(8,128)} copy(f32[4,8,64,64]{2,3,1,0:T(8,128)} %get-tuple-element.22) | data formatting | bytes 1048576 | tf_op jit(solution)/shard_map/transpose(jvp())/add_any | solution.py:35
  150.3 1.9 fusion.11
  152.1 5.1 %all-to-all-start.6 = ((bf16[4,128,256]{1,2,0:T(8,128)(2,1)}), bf16[4,128,256]{1,2,0:T(8,128)(2,1)}, u32[]{:S(2)}, u32[]{:S(2)}) async-start(bf16[4,128,256]{1,2,0:T(8,128)(2,1)} %copy.226), calls=%async_computation.6 | async-start | bytes 524288 | tf_op jit(solution)/shard_map/all_to_all | solution.py:104
  157.2 2.3 %fusion.47 = f32[4,8,64,64]{3,1,2,0:T(8,128)S(1)} fusion(f32[4,8,64,64]{3,1,2,0:T(8,128)} %copy.246), kind=kOutput, calls=%fused_computation.85 | output fusion | flops 8257536 | bytes 1048576 | tf_op jit(solution)/shard_map/transpose(jvp(jit(cumsum)))/reduce_window_sum | solution.py:34
  159.5 1.4 copy.247
  160.9 1.6 reshape.163
  165.0 5.2 %all-to-all-start.7 = ((bf16[4,128,512]{2,1,0:T(8,128)(2,1)}), bf16[4,128,512]{2,1,0:T(8,128)(2,1)S(1)}, u32[]{:S(2)}, u32[]{:S(2)}) async-start(bf16[4,128,512]{2,1,0:T(8,128)(2,1)} %convert_element_type.84), calls=%async_computation.7 | async-start | bytes 1048576 | tf_op jit(solution)/shard_map/all_to_all | solution.py:107
  172.6 1.6 collective-permute-start.1
  174.2 2.8 %collective-permute-done.1 = f32[64,256]{1,0:T(8,128)S(1)} collective-permute-done((f32[64,256]{1,0:T(8,128)S(1)}, f32[64,256]{1,0:T(8,128)S(1)}, u32[]{:S(2)}, u32[]{:S(2)}) %collective-permute-start.1) | collective-permute-done | bytes 65568 | tf_op jit(solution)/shard_map/ppermute | solution.py:124
  177.0 1.6 collective-permute-start.2
  178.6 2.7 %collective-permute-done.2 = f32[64,256]{1,0:T(8,128)S(1)} collective-permute-done((f32[64,256]{1,0:T(8,128)S(1)}, f32[64,256]{1,0:T(8,128)S(1)}, u32[]{:S(2)}, u32[]{:S(2)}) %collective-permute-start.2) | collective-permute-done | bytes 65568 | tf_op jit(solution)/shard_map/ppermute | solution.py:124
  181.3 15.3 %all_gather.7 = f32[64,1024]{1,0:T(8,128)S(1)} all-gather(f32[64,256]{1,0:T(8,128)S(1)} %add.52), channel_id=1, replica_groups=mesh['sp'=4,'dp'=8] {'sp'}, dimensions={1}, use_global_device_ids=true | all-gather | bytes 327680 | tf_op jit(solution)/shard_map/all_gather | solution.py:125
  196.6 1.4 convert_element_type.86
  198.9 1.8 copy.249
  200.9 1.0 copy.250
  (122 shorter events, 24.5 us)
Async XLA Ops:
  7.2 41.7 %copy-start = (bf16[64,1024]{1,0:T(8,128)(2,1)S(1)}, bf16[64,1024]{1,0:T(8,128)(2,1)}, u32[]{:S(2)}) copy-start(bf16[64,1024]{1,0:T(8,128)(2,1)} %param.13) | copy-start | bytes 393220
  7.2 12.1 %all-to-all-start.1 = ((bf16[128,4,4]{0,2,1:T(4,128)(2,1)}), bf16[128,4,4]{0,2,1:T(4,128)(2,1)S(1)}, u32[]{:S(2)}, u32[]{:S(2)}) async-start(bf16[128,4,4]{0,2,1:T(4,128)(2,1)} %bitcast.168), calls=%async_computation.1 | async-start | bytes 8192 | tf_op jit(solution)/shard_map/all_to_all | solution.py:75
  19.3 3.6 %copy-start.20 = (bf16[128,1024]{1,0:T(8,128)(2,1)S(1)}, bf16[128,1024]{1,0:T(8,128)(2,1)}, u32[]{:S(2)}) copy-start(bf16[128,1024]{1,0:T(8,128)(2,1)} %param.9) | copy-start | bytes 786436
  19.3 11.4 %all-to-all-start.5 = ((bf16[128,4,256]{0,2,1:T(8,128)(2,1)}), bf16[128,4,256]{0,2,1:T(8,128)(2,1)S(1)}, u32[]{:S(2)}, u32[]{:S(2)}) async-start(bf16[128,4,256]{0,2,1:T(8,128)(2,1)} %bitcast.24), calls=%async_computation.5 | async-start | bytes 524288 | tf_op jit(solution)/shard_map/all_to_all | solution.py:71
  22.8 11.3 %copy-start.17 = (bf16[128,2048]{1,0:T(8,128)(2,1)S(1)}, bf16[128,2048]{1,0:T(8,128)(2,1)}, u32[]{:S(2)}) copy-start(bf16[128,2048]{1,0:T(8,128)(2,1)} %param.11) | copy-start | bytes 1572868
  30.7 19.4 %all-to-all-start = ((bf16[128,4,256]{0,2,1:T(8,128)(2,1)}), bf16[128,4,256]{0,2,1:T(8,128)(2,1)S(1)}, u32[]{:S(2)}, u32[]{:S(2)}) async-start(bf16[128,4,256]{0,2,1:T(8,128)(2,1)} %bitcast), calls=%async_computation | async-start | bytes 524288 | tf_op jit(solution)/shard_map/all_to_all | solution.py:72
  34.1 1.6 copy-start.31
  48.2 1.9 copy-start.21
  50.1 0.7 copy-start.15
  50.1 5.4 %copy-start.18 = (bf16[128,2048]{1,0:T(8,128)(2,1)S(1)}, bf16[128,2048]{1,0:T(8,128)(2,1)}, u32[]{:S(2)}) copy-start(bf16[128,2048]{1,0:T(8,128)(2,1)} %param.10) | copy-start | bytes 1572868
  50.8 32.2 %all-to-all-start.3 = ((bf16[128,4,512]{2,0,1:T(8,128)(2,1)}), bf16[128,4,512]{2,0,1:T(8,128)(2,1)}, u32[]{:S(2)}, u32[]{:S(2)}) async-start(bf16[128,4,512]{2,0,1:T(8,128)(2,1)} %bitcast.143), calls=%async_computation.3 | async-start | bytes 1048576 | tf_op jit(solution)/shard_map/all_to_all | solution.py:74
  83.1 15.5 %all-to-all-start.2 = ((bf16[128,4,512]{2,0,1:T(8,128)(2,1)}), bf16[128,4,512]{2,0,1:T(8,128)(2,1)}, u32[]{:S(2)}, u32[]{:S(2)}) async-start(bf16[128,4,512]{2,0,1:T(8,128)(2,1)} %bitcast.144), calls=%async_computation.2 | async-start | bytes 1048576 | tf_op jit(solution)/shard_map/all_to_all | solution.py:73
  90.6 1.0 copy-start.16
  100.5 1.2 copy-start.1
  101.7 7.0 %copy-start.5 = (bf16[4,512,128]{2,1,0:T(8,128)(2,1)}, bf16[4,512,128]{2,1,0:T(8,128)(2,1)S(1)}, u32[]{:S(2)}) copy-start(bf16[4,512,128]{2,1,0:T(8,128)(2,1)S(1)} %copy.198) | copy-start | bytes 1572868
  101.7 1.1 copy-start.23
  101.7 1.1 copy-start.24
  101.7 1.1 copy-start.32
  105.8 2.9 %copy-start.8 = (f32[8,4,64,128]{3,0,2,1:T(8,128)}, f32[8,4,64,128]{3,0,2,1:T(8,128)S(1)}, u32[]{:S(2)}) copy-start(f32[8,4,64,128]{3,0,2,1:T(8,128)S(1)} %convolution_bitcast_fusion) | copy-start | bytes 3145732
  108.6 1.0 copy-start.3
  116.4 2.0 copy-start.26
  118.4 0.9 copy-start.25
  119.3 0.7 copy-start.30
  121.4 1.4 copy-start.29
  122.8 1.4 copy-start.27
  125.8 1.3 copy-start.11
  125.9 1.5 copy-start.12
  125.9 1.8 copy-start.13
  127.7 1.5 copy-start.7
  127.7 1.5 copy-start.10
  138.0 4.9 %copy-start.28 = (pred[64,64]{1,0:T(8,128)(4,1)S(1)}, pred[64,64]{1,0:T(8,128)(4,1)}, u32[]{:S(2)}) copy-start(pred[64,64]{1,0:T(8,128)(4,1)} %iota_compare_fusion) | copy-start | bytes 12292
  138.0 14.2 %all-to-all-start.4 = ((bf16[4,128,256]{1,2,0:T(8,128)(2,1)}), bf16[4,128,256]{1,2,0:T(8,128)(2,1)S(1)}, u32[]{:S(2)}, u32[]{:S(2)}) async-start(bf16[4,128,256]{1,2,0:T(8,128)(2,1)} %copy.213), calls=%async_computation.4 | async-start | bytes 524288 | tf_op jit(solution)/shard_map/all_to_all | solution.py:101
  146.0 2.7 %copy-start.14 = (bf16[4,8,64,64]{2,3,1,0:T(8,128)(2,1)S(1)}, bf16[4,8,64,64]{2,3,1,0:T(8,128)(2,1)}, u32[]{:S(2)}) copy-start(bf16[4,8,64,64]{2,3,1,0:T(8,128)(2,1)} %get-tuple-element.23) | copy-start | bytes 786436
  148.6 1.5 copy-start.9
  149.0 1.3 copy-start.4
  152.1 12.9 %all-to-all-start.6 = ((bf16[4,128,256]{1,2,0:T(8,128)(2,1)}), bf16[4,128,256]{1,2,0:T(8,128)(2,1)}, u32[]{:S(2)}, u32[]{:S(2)}) async-start(bf16[4,128,256]{1,2,0:T(8,128)(2,1)} %copy.226), calls=%async_computation.6 | async-start | bytes 524288 | tf_op jit(solution)/shard_map/all_to_all | solution.py:104
  160.9 1.6 copy-start.2
  160.9 1.7 copy-start.6
  165.0 5.2 %copy-start.19 = (f32[256,512]{1,0:T(8,128)S(1)}, f32[256,512]{1,0:T(8,128)}, u32[]{:S(2)}) copy-start(f32[256,512]{1,0:T(8,128)} %get-tuple-element.30) | copy-start | bytes 1572868
  165.0 35.6 %all-to-all-start.7 = ((bf16[4,128,512]{2,1,0:T(8,128)(2,1)}), bf16[4,128,512]{2,1,0:T(8,128)(2,1)S(1)}, u32[]{:S(2)}, u32[]{:S(2)}) async-start(bf16[4,128,512]{2,1,0:T(8,128)(2,1)} %convert_element_type.84), calls=%async_computation.7 | async-start | bytes 1048576 | tf_op jit(solution)/shard_map/all_to_all | solution.py:107
  170.3 26.4 %reduce-scatter.2.cloned.1.call-start = ((), (), s32[]{:S(2)}) async-start(), calls=%async_computation.9 | async-start | bytes 163840 | tf_op jit(solution)/shard_map/reduce_scatter | solution.py:116
  170.3 0.8 copy-start.22
  171.3 1.3 collective-permute-start
  172.6 4.3 %collective-permute-start.1 = (f32[64,256]{1,0:T(8,128)S(1)}, f32[64,256]{1,0:T(8,128)S(1)}, u32[]{:S(2)}, u32[]{:S(2)}) collective-permute-start(f32[64,256]{1,0:T(8,128)S(1)} %add.50), channel_id=1, source_target_pairs={{0,2},{1,3},{2,0},{3,1},{4,6},{5,7},{6,4},{7,5},{8,10},{9,11},{10,... | collective-permute-start | bytes 196616 | tf_op jit(solution)/shard_map/ppermute | solution.py:124
  177.0 4.3 %collective-permute-start.2 = (f32[64,256]{1,0:T(8,128)S(1)}, f32[64,256]{1,0:T(8,128)S(1)}, u32[]{:S(2)}, u32[]{:S(2)}) collective-permute-start(f32[64,256]{1,0:T(8,128)S(1)} %add.51), channel_id=1, source_target_pairs={{0,4},{1,5},{2,6},{3,7},{4,0},{5,1},{6,2},{7,3},{8,12},{9,13},{10,... | collective-permute-start | bytes 196616 | tf_op jit(solution)/shard_map/ppermute | solution.py:124
Sparse Core Ops, SparseCore 0:
  173.9 21.1 reduce-scatter.1
